TPU v7x, 512 devices: a 4x2x32 block of a 4x8x32 slice. The times are simulated.
512 devices in a mesh: grp: 2 (over y), fs: 32 (over z), tp: 8 (over x, core).
Axes of the slice: x: 4, y: 2, z: 32, core: 2. Of those that a mesh axis runs over, the one named last changes fastest.
The devices are a block of a 4x8x32 slice.
Arguments:
- tokens: bfloat16 [32768, 2048], P(('grp', 'fs')), parts along dimension 0, may hold values from -6 to 6
- pre_gain: float32 [2048], replicated, may hold values from 0.1 to 1.9
- up_weight: float32 [2048, 8192], P('fs', 'tp'), may hold values from -0.125 to 0.125
- up_scale: float32 [8192], P('tp'), may hold values from 0.3 to 3
- down_weight: float32 [8192, 2048], P('tp', 'fs'), may hold values from -0.0625 to 0.0625
- down_scale: float32 [2048], P('fs'), may hold values from 0.3 to 3
- post_gain: float32 [2048], replicated, may hold values from 0.1 to 1.9
Outputs:
- mixed: bfloat16 [32768, 2048], P(('grp', 'fs')), parts along dimension 0
There are 2 independent parts, one for each index of `grp`. A program takes and returns all parts, laid end to end along the dimension named above; an argument that names none is the same for every part. Nothing has to cross between parts.
All inputs are finite; a program needn't handle non-finite values.
Results may differ from a plain program's by a relative error of at most 0.01.
Values may be sent and summed in bfloat16 or wider, within the bound.
A program may use at most 64 MiB of HBM per device.

v0:
```python
import jax
import jax.numpy as jnp
from jax import lax
from jax.sharding import PartitionSpec as P

epsilon = 1e-06


def joined_along(parts, dim):
    shape = list(parts.shape[1:])
    shape[dim] *= parts.shape[0]
    return jnp.moveaxis(parts, 0, dim).reshape(shape)


def sent_to_all(shard, axis):
    length = lax.axis_size(axis)
    return lax.all_to_all(
        jnp.broadcast_to(shard[None], (length, *shard.shape)), axis, 0, 0, tiled=True
    )


def gathered_copies(shard, axis, dim):
    return joined_along(sent_to_all(shard, axis), dim)


def turned_gather(arrays, axis, dims):
    turned = [jnp.moveaxis(a, dim, 0) for a, dim in zip(arrays, dims)]
    widths = [t[0].size for t in turned]
    both = jnp.concatenate([t.reshape(-1, w) for t, w in zip(turned, widths)], axis=1)
    whole = lax.all_gather(both, axis, axis=0, tiled=True)
    parts = jnp.split(whole, [sum(widths[:k]) for k in range(1, len(widths))], axis=1)
    return tuple(
        (
            jnp.moveaxis(b.reshape(-1, *t.shape[1:]), 0, dim)
            for b, t, dim in zip(parts, turned, dims)
        )
    )


def in_blocks(shard, dim, length):
    before, after = (shard.shape[:dim], shard.shape[dim + 1 :])
    return jnp.moveaxis(shard.reshape(*before, length, -1, *after), dim, 0)


def summed_on_arrival(shard, axis, dim):
    parts = in_blocks(shard, dim, lax.axis_size(axis))
    arrived = lax.all_to_all(parts, axis, split_axis=0, concat_axis=0, tiled=True)
    return arrived.astype(jnp.float32).sum(axis=0)


def rms_rows(values, scaling):
    return values * lax.rsqrt(jnp.mean(values * values, axis=-1, keepdims=True) + epsilon) * scaling


def activate(lifted, up_scale):
    return jnp.square(jax.nn.relu(lifted * up_scale)).astype(jnp.bfloat16)


def on_device(tokens, pre_gain, up_weight, up_scale, down_weight, down_scale, post_gain):
    residual = tokens.astype(jnp.float32)
    normed = rms_rows(residual, pre_gain).astype(jnp.bfloat16)
    up_cast = up_weight.astype(jnp.bfloat16)
    down_cast = down_weight.astype(jnp.bfloat16)
    column_scales = gathered_copies(down_scale, "fs", 0)
    up_full, down_full = turned_gather((up_cast, down_cast), "fs", (0, 1))
    lifted = jnp.dot(normed, up_full, preferred_element_type=jnp.float32)
    hidden = activate(lifted, up_scale)
    partials = jnp.dot(hidden, down_full, preferred_element_type=jnp.float32)
    partials = (partials * column_scales).astype(jnp.bfloat16)
    summed = summed_on_arrival(partials, "tp", 0)
    branch = lax.optimization_barrier(summed.astype(jnp.bfloat16)).astype(jnp.float32)
    row_count = branch.shape[0]
    offset = lax.axis_index("tp") * row_count
    own_rows = lax.dynamic_slice_in_dim(residual, offset, row_count, 0)
    result = (own_rows + rms_rows(branch, post_gain)).astype(jnp.bfloat16)
    return gathered_copies(result, "tp", 0)


def solution(mesh):
    placed = (P(("grp", "fs"), None), P(), P("fs", "tp"), P("tp"), P("tp", "fs"), P("fs"), P())
    return jax.shard_map(
        on_device, mesh=mesh, in_specs=placed, out_specs=P(("grp", "fs"), None), check_vma=False
    )
```

profile of v0, /device:TPU:33, one launch (start us, length us, event | category | flops | bytes accessed | tf_op | source)
XLA Modules:
  0.0 268.8 jit_solution(17365989303714553077)
XLA Ops:
  6.5 0.0 all-gather.2.cloned.1.call-start
  6.6 1.0 convert_bitcast_fusion
  7.5 1.0 convert_element_type.28
  8.5 0.7 pad_maximum_fusion
  9.2 0.1 all-gather.2.cloned.1.call-update
  9.3 1.3 broadcast_in_dim.4
  10.5 46.3 %all-to-all-start = ((f32[32,1,64]{2,1,0:T(1,128)}), f32[32,1,64]{2,1,0:T(1,128)S(1)}, u32[]{:S(2)}, u32[]{:S(2)}) async-start(f32[32,1,64]{2,1,0:T(1,128)} %broadcast_in_dim.4), calls=%async_computation | async-start | bytes 32768 | tf_op jit(solution)/shard_map/all_to_all | solution.py:17
  56.8 2.1 multiply_reduce_fusion
  58.9 18.4 %all-to-all-done = f32[32,1,64]{2,1,0:T(1,128)S(1)} async-done(((f32[32,1,64]{2,1,0:T(1,128)}), f32[32,1,64]{2,1,0:T(1,128)S(1)}, u32[]{:S(2)}, u32[]{:S(2)}) %all-to-all-start) | async-done | bytes 8224 | tf_op jit(solution)/shard_map/all_to_all | solution.py:17
  77.4 0.5 broadcast.32
  77.9 0.6 reduce.4
  78.5 0.1 mul.67
  78.5 88.1 %all-gather.2.cloned.1.call-done = bf16[2048,2048]{1,0:T(8,128)(2,1)} async-done(((bf16[64,2048]{1,0:T(8,128)(2,1)}), bf16[2048,2048]{1,0:T(8,128)(2,1)}) %all-gather.2.cloned.1.call-update) | async-done | bytes 8388624 | tf_op jit(solution)/shard_map/all_gather | solution.py:30
  166.6 9.9 %multiply_convert_fusion = bf16[512,2048]{1,0:T(8,128)(2,1)} fusion(bf16[2048,2048]{1,0:T(8,128)(2,1)} %all-gather.2.cloned.1.call-done, f32[2048]{0:T(1024)S(1)} %mul.67, f32[2048]{0:T(1024)} %param.8, f32[512]{0:T(512)S(1)} %add_rsqrt_fusion, bf16[512,2048]{1,0:T(8,128)(2,1)} %param.7, f32[1024]{0:T(1024)} %param.10), kind=kOutput, calls=%fused_computation.4 | convolution fusion | flops 4303355904 | bytes 12605440 | tf_op jit(solution)/shard_map/dot_general | solution.py:68
  176.6 0.0 copy-start
  176.6 24.5 %all-to-all-start.1 = ((bf16[8,64,2048]{2,1,0:T(8,128)(2,1)}), bf16[8,64,2048]{2,1,0:T(8,128)(2,1)}, u32[]{:S(2)}, u32[]{:S(2)}) async-start(bf16[8,64,2048]{2,1,0:T(8,128)(2,1)} %bitcast.5), calls=%async_computation.1 | async-start | bytes 4194304 | tf_op jit(solution)/shard_map/all_to_all | solution.py:47
  201.1 0.0 copy-done
  201.1 0.0 copy-start.1
  201.1 2.5 convert_element_type.26
  203.5 23.9 %all-to-all-done.1 = bf16[8,64,2048]{2,1,0:T(8,128)(2,1)} async-done(((bf16[8,64,2048]{2,1,0:T(8,128)(2,1)}), bf16[8,64,2048]{2,1,0:T(8,128)(2,1)}, u32[]{:S(2)}, u32[]{:S(2)}) %all-to-all-start.1) | async-done | bytes 2097184 | tf_op jit(solution)/shard_map/all_to_all | solution.py:47
  227.4 2.0 reduce_sum.31
  229.3 0.2 fusion.15
  229.5 0.0 copy-done.1
  229.5 1.2 fusion.18
  230.7 0.2 broadcast_in_dim.5
  231.0 29.7 %all_to_all.16 = bf16[8,64,2048]{2,1,0:T(8,128)(2,1)S(1)} all-to-all(bf16[8,64,2048]{2,1,0:T(8,128)(2,1)S(1)} %broadcast_in_dim.5), channel_id=1, replica_groups=mesh['grp'=2,'fs'=32,'tp'=8] {'tp'}, dimensions={0} | all-to-all | bytes 4194304 | tf_op jit(solution)/shard_map/all_to_all | solution.py:17
  260.6 1.3 copy.9
  (2 shorter events, 0.0 us)
Async XLA Ops:
  6.5 160.1 %all-gather.2.cloned.1.call-start = ((), (), s32[]{:S(2)}) async-start(), calls=%async_computation.3 | async-start | bytes 8650752 | tf_op jit(solution)/shard_map/all_gather | solution.py:30
  10.5 66.8 %all-to-all-start = ((f32[32,1,64]{2,1,0:T(1,128)}), f32[32,1,64]{2,1,0:T(1,128)S(1)}, u32[]{:S(2)}, u32[]{:S(2)}) async-start(f32[32,1,64]{2,1,0:T(1,128)} %broadcast_in_dim.4), calls=%async_computation | async-start | bytes 32768 | tf_op jit(solution)/shard_map/all_to_all | solution.py:17
  176.6 24.5 %copy-start = (bf16[512,2048]{1,0:T(8,128)(2,1)S(1)}, bf16[512,2048]{1,0:T(8,128)(2,1)}, u32[]{:S(2)}) copy-start(bf16[512,2048]{1,0:T(8,128)(2,1)} %param.7) | copy-start | bytes 6291460
  176.6 50.8 %all-to-all-start.1 = ((bf16[8,64,2048]{2,1,0:T(8,128)(2,1)}), bf16[8,64,2048]{2,1,0:T(8,128)(2,1)}, u32[]{:S(2)}, u32[]{:S(2)}) async-start(bf16[8,64,2048]{2,1,0:T(8,128)(2,1)} %bitcast.5), calls=%async_computation.1 | async-start | bytes 4194304 | tf_op jit(solution)/shard_map/all_to_all | solution.py:47
  201.1 28.4 %copy-start.1 = (f32[2048]{0:T(1024)S(1)}, f32[2048]{0:T(1024)}, u32[]{:S(2)}) copy-start(f32[2048]{0:T(1024)} %param.13) | copy-start | bytes 24580
Sparse Core Ops, SparseCore 0:
  9.4 157.1 all-gather.1
where the time goes:
time: 269 us
  waiting for transfers between devices  130 us (48%)
  starting transfers between devices  70.8 us (26%)
  blocking collectives  29.7 us (11%)
  between operations  13.5 us (5%)
  other arithmetic  11.1 us (4%)
  matrix products  9.94 us (4%)
  local copies, waits for them, and re-layouts  3.39 us (1%)
    all_gather x1, waiting for transfers between devices, turned_gather(): whole = lax.all_gather(both, axis, axis=0, tiled=True)  88.1 us
    all_to_all x1, starting transfers between devices, sent_to_all(): lax.all_to_all(jnp.broadcast_to(shard[None], (length, *shard.shape)), axi...  46.3 us
    all_to_all x1, blocking collectives, sent_to_all(): lax.all_to_all(jnp.broadcast_to(shard[None], (length, *shard.shape)), axi...  29.7 us
    all_to_all x1, starting transfers between devices, summed_on_arrival(): lax.all_to_all(parts, axis, split_axis=0, concat_axis=0, tiled=True)  24.5 us
    all_to_all x1, waiting for transfers between devices, summed_on_arrival(): lax.all_to_all(parts, axis, split_axis=0, concat_axis=0, tiled=True)  23.9 us
    all_to_all x1, waiting for transfers between devices, sent_to_all(): lax.all_to_all(jnp.broadcast_to(shard[None], (length, *shard.shape)), axi...  18.4 us
    dot_general x1, matrix products, on_device(): partials = jnp.dot(hidden, down_full, preferred_element_type=jnp.float32)  9.94 us
  transfers between devices with their start and end apart: 3, of which 3 were waited for; matrix products, arithmetic and copies ran while one was open for 3% of the time, Pallas kernels for 0%

commit v1 on v0

--- a/solution.py
+++ b/solution.py
@@ -27,7 +27,8 @@
     turned = [jnp.moveaxis(a, dim, 0) for a, dim in zip(arrays, dims)]
     widths = [t[0].size for t in turned]
     both = jnp.concatenate([t.reshape(-1, w) for t, w in zip(turned, widths)], axis=1)
-    whole = lax.all_gather(both, axis, axis=0, tiled=True)
+    outgoing = jnp.stack([both] * lax.axis_size(axis))
+    whole = jnp.concatenate(lax.all_to_all(outgoing, axis, 0, 0), axis=0)
     parts = jnp.split(whole, [sum(widths[:k]) for k in range(1, len(widths))], axis=1)
     return tuple(
         (

time: 269 us -> 886 us (3.29)
  the two profiles are of different devices: /device:TPU:33 before, /device:TPU:224 now
where the time goes in v1:
time: 886 us
  waiting for transfers between devices  775 us (87%)
  starting transfers between devices  54.5 us (6%)
  blocking collectives  29.7 us (3%)
  matrix products  9.35 us (1%)
  other arithmetic  8.91 us (1%)
    all_to_all x1, waiting for transfers between devices, turned_gather(): whole = jnp.concatenate(lax.all_to_all(outgoing, axis, 0, 0), axis=0)  733 us
    all_to_all x1, starting transfers between devices, sent_to_all(): lax.all_to_all(jnp.broadcast_to(shard[None], (length, *shard.shape)), axi...  41.7 us
    all_to_all x1, blocking collectives, sent_to_all(): lax.all_to_all(jnp.broadcast_to(shard[None], (length, *shard.shape)), axi...  29.7 us
    all_to_all x1, waiting for transfers between devices, summed_on_arrival(): lax.all_to_all(parts, axis, split_axis=0, concat_axis=0, tiled=True)  24.8 us
  transfers between devices with their start and end apart: 3, of which 3 were waited for; matrix products, arithmetic and copies ran while one was open for 1% of the time, Pallas kernels for 0%

profile of v1, /device:TPU:224, one launch (start us, length us, event | category | flops | bytes accessed | tf_op | source)
XLA Modules:
  0.0 885.5 jit_solution(14603014351865717425)
XLA Ops:
  0.0 1.3 broadcast_in_dim.4
  1.3 41.7 %all-to-all-start.1 = ((f32[32,1,64]{2,1,0:T(1,128)}), f32[32,1,64]{2,1,0:T(1,128)S(1)}, u32[]{:S(2)}, u32[]{:S(2)}) async-start(f32[32,1,64]{2,1,0:T(1,128)} %broadcast_in_dim.4), calls=%async_computation.1 | async-start | bytes 32768 | tf_op jit(solution)/shard_map/all_to_all | solution.py:17
  43.0 1.0 convert_bitcast_fusion
  43.9 1.0 convert_element_type.28
  44.9 17.0 %all-to-all-done.1 = f32[32,1,64]{2,1,0:T(1,128)S(1)} async-done(((f32[32,1,64]{2,1,0:T(1,128)}), f32[32,1,64]{2,1,0:T(1,128)S(1)}, u32[]{:S(2)}, u32[]{:S(2)}) %all-to-all-start.1) | async-done | bytes 8224 | tf_op jit(solution)/shard_map/all_to_all | solution.py:17
  62.0 4.3 stack.2
  66.2 0.0 copy-start
  66.2 0.0 copy-start.2
  66.3 0.0 copy-start.3
  66.3 8.2 all-to-all-start
  74.5 0.0 copy-done
  74.5 0.5 multiply_reduce_fusion
  75.0 0.5 broadcast.34
  75.5 0.7 reduce.4
  76.2 0.1 mul.67
  76.2 733.4 %all-to-all-done = bf16[32,64,2048]{2,1,0:T(8,128)(2,1)} async-done(((bf16[32,64,2048]{2,1,0:T(8,128)(2,1)}), bf16[32,64,2048]{2,1,0:T(8,128)(2,1)}, u32[]{:S(2)}, u32[]{:S(2)}) %all-to-all-start) | async-done | bytes 8388640 | tf_op jit(solution)/shard_map/all_to_all | solution.py:31
  809.7 0.0 copy-done.2
  809.7 0.0 copy-done.3
  809.7 9.4 %multiply_convert_fusion = bf16[512,2048]{1,0:T(8,128)(2,1)} fusion(bf16[2048,2048]{1,0:T(8,128)(2,1)} %bitcast.1, f32[2048]{0:T(1024)S(1)} %mul.67, f32[2048]{0:T(1024)S(1)} %copy-done.2, f32[512]{0:T(512)S(1)} %add_rsqrt_fusion, bf16[512,2048]{1,0:T(8,128)(2,1)S(1)} %copy-done, f32[1024]{0:T(1024)S(1)} %copy-done.3), kind=kOutput, calls=%fused_computation.4 | convolution fusion | flops 4303355904 | bytes 12605440 | tf_op jit(solution)/shard_map/dot_general | solution.py:69
  819.0 4.6 all-to-all-start.2
  823.6 0.0 copy-start.1
  823.6 2.5 convert_element_type.26
  826.1 24.8 %all-to-all-done.2 = bf16[8,64,2048]{2,1,0:T(8,128)(2,1)} async-done(((bf16[8,64,2048]{2,1,0:T(8,128)(2,1)}), bf16[8,64,2048]{2,1,0:T(8,128)(2,1)}, u32[]{:S(2)}, u32[]{:S(2)}) %all-to-all-start.2) | async-done | bytes 2097184 | tf_op jit(solution)/shard_map/all_to_all | solution.py:48
  850.9 2.0 reduce_sum.31
  852.9 0.2 fusion.15
  853.0 0.0 copy-done.1
  853.0 1.2 fusion.18
  854.2 0.2 broadcast_in_dim.5
  854.5 29.7 %all_to_all.21 = bf16[8,64,2048]{2,1,0:T(8,128)(2,1)S(1)} all-to-all(bf16[8,64,2048]{2,1,0:T(8,128)(2,1)S(1)} %broadcast_in_dim.5), channel_id=1, replica_groups=mesh['grp'=2,'fs'=32,'tp'=8] {'tp'}, dimensions={0} | all-to-all | bytes 4194304 | tf_op jit(solution)/shard_map/all_to_all | solution.py:17
  884.2 1.3 copy.9
  (3 shorter events, 0.0 us)
Async XLA Ops:
  1.3 60.7 %all-to-all-start.1 = ((f32[32,1,64]{2,1,0:T(1,128)}), f32[32,1,64]{2,1,0:T(1,128)S(1)}, u32[]{:S(2)}, u32[]{:S(2)}) async-start(f32[32,1,64]{2,1,0:T(1,128)} %broadcast_in_dim.4), calls=%async_computation.1 | async-start | bytes 32768 | tf_op jit(solution)/shard_map/all_to_all | solution.py:17
  66.2 8.2 copy-start
  66.2 743.4 %copy-start.2 = (f32[2048]{0:T(1024)S(1)}, f32[2048]{0:T(1024)}, u32[]{:S(2)}) copy-start(f32[2048]{0:T(1024)} %param.8) | copy-start | bytes 24580
  66.3 743.4 %copy-start.3 = (f32[1024]{0:T(1024)S(1)}, f32[1024]{0:T(1024)}, u32[]{:S(2)}) copy-start(f32[1024]{0:T(1024)} %param.10) | copy-start | bytes 12292
  66.3 743.4 %all-to-all-start = ((bf16[32,64,2048]{2,1,0:T(8,128)(2,1)}), bf16[32,64,2048]{2,1,0:T(8,128)(2,1)}, u32[]{:S(2)}, u32[]{:S(2)}) async-start(bf16[32,64,2048]{2,1,0:T(8,128)(2,1)} %stack.2), calls=%async_computation | async-start | bytes 16777216 | tf_op jit(solution)/shard_map/all_to_all | solution.py:31
  819.0 31.9 %all-to-all-start.2 = ((bf16[8,64,2048]{2,1,0:T(8,128)(2,1)}), bf16[8,64,2048]{2,1,0:T(8,128)(2,1)}, u32[]{:S(2)}, u32[]{:S(2)}) async-start(bf16[8,64,2048]{2,1,0:T(8,128)(2,1)} %bitcast.6), calls=%async_computation.2 | async-start | bytes 4194304 | tf_op jit(solution)/shard_map/all_to_all | solution.py:48
  823.6 29.4 %copy-start.1 = (f32[2048]{0:T(1024)S(1)}, f32[2048]{0:T(1024)}, u32[]{:S(2)}) copy-start(f32[2048]{0:T(1024)} %param.13) | copy-start | bytes 24580
